TPU v7x, 256 devices: a whole 4x4x8 slice. The times are simulated.
256 devices in a mesh: ep: 64 (over z, x, core), tp: 4 (over y).
Axes of the slice: x: 4, y: 4, z: 8, core: 2. Of those that a mesh axis runs over, the one named last changes fastest.
Arguments:
- mixer_input: bfloat16 [40960, 2048], P('ep'), may hold values from -6 to 6
- mixer_gain: float32 [2048], replicated, may hold values from 0.1 to 1.9
- value_weight: bfloat16 [2048, 1024], P(None, 'tp'), may hold values from -0.125 to 0.125
- inner_gate: bfloat16 [2048, 1024], P(None, 'tp'), may hold values from -0.125 to 0.125
- outer_gate: bfloat16 [2048, 1024], P(None, 'tp'), may hold values from -0.125 to 0.125
- kernel_taps: float32 [3, 1024], P(None, 'tp'), may hold values from -3 to 3
- mixer_proj: bfloat16 [1024, 2048], P('tp'), may hold values from -0.1875 to 0.1875
- expert_input: bfloat16 [40960, 2048], P(('ep', 'tp')), may hold values from -6 to 6
- expert_gain: float32 [2048], replicated, may hold values from 0.1 to 1.9
- routes: int32 [40960, 2], P(('ep', 'tp')), may hold values from 0 to 63, as said below
- group_logits: float32 [40960, 8], P(('ep', 'tp')), may hold values from -6 to 6
- pair_logits: float32 [40960, 2], P(('ep', 'tp')), may hold values from -6 to 6
- gate_weight: bfloat16 [64, 2048, 1024], P('ep', None, 'tp'), may hold values from -0.125 to 0.125
- up_weight: bfloat16 [64, 2048, 1024], P('ep', None, 'tp'), may hold values from -0.125 to 0.125
- down_weight: bfloat16 [64, 1024, 2048], P('ep', 'tp'), may hold values from -0.75 to 0.75
Outputs:
- mixer_output: bfloat16 [40960, 2048], P(('ep', 'tp'))
- expert_output: bfloat16 [40960, 2048], P(('ep', 'tp'))
Inputs may be any that keep to these rules, and one draw needn't show every extreme that they name: `routes`: both entries of a row are different experts of one group (equal after integer division by 8). In the rows of one device every group is chosen by the same number of rows, no expert is named more than 10 times, and in every draw one expert is named exactly 10 times in the rows of every device.
All inputs are finite; a program needn't handle non-finite values.
Results may differ from a plain program's by a relative error of at most 0.01.
Values may be sent and summed in bfloat16 or wider, within the bound.
A program may use at most 128 MiB of HBM per device.

v0:
```python
import jax
import jax.numpy as jnp
from jax import lax
from jax.sharding import PartitionSpec as P

EPG = 8
EPSILON = 1e-06


def padded_2(cells, axis):
    count = lax.axis_size(axis)
    ends = count - 1
    head = cells[:1]
    tail = cells[-1:]
    return jnp.concatenate(
        [
            lax.ppermute(tail, axis, [(i, i + 1) for i in range(ends)]),
            cells,
            lax.ppermute(head, axis, [(i + 1, i) for i in range(ends)]),
        ],
        axis=0,
    )


def normed(values, gain):
    wide = values.astype(jnp.float32)
    scale = lax.rsqrt(jnp.mean(wide * wide, axis=-1, keepdims=True) + EPSILON)
    return (wide * scale * gain).astype(jnp.bfloat16)


def route_weights(routes, group_logits, pair_logits):
    chosen = routes[:, 0] // EPG
    groups = jnp.arange(group_logits.shape[1], dtype=jnp.int32)
    picked = jnp.sum(jnp.where(groups[None, :] == chosen[:, None], group_logits, 0.0), axis=1)
    group_weight = 1.0 / jnp.sum(jnp.exp(group_logits - picked[:, None]), axis=1)
    return group_weight[:, None] * jax.nn.sigmoid(pair_logits - pair_logits[:, ::-1])


def f32dot(a, b):
    return jnp.dot(a, b, preferred_element_type=jnp.float32)


def on_device(
    mixer_input,
    mixer_gain,
    value_weight,
    inner_gate,
    outer_gate,
    kernel_taps,
    mixer_proj,
    expert_input,
    expert_gain,
    routes,
    group_logits,
    pair_logits,
    gate_weight,
    up_weight,
    down_weight,
):
    split = lax.axis_size("tp")
    experts = lax.axis_size("ep")
    n_groups = experts // EPG
    local = expert_input.shape[0]
    width = expert_input.shape[1]
    per = local // n_groups
    expert_norm = normed(expert_input, expert_gain)
    weights = route_weights(routes, group_logits, pair_logits)
    member = routes % EPG
    lanes = jnp.arange(EPG, dtype=jnp.int32)
    wide_w = jnp.where(member[:, 0:1] == lanes, weights[:, 0:1], 0.0) + jnp.where(
        member[:, 1:2] == lanes, weights[:, 1:2], 0.0
    )
    high = wide_w.astype(jnp.bfloat16)
    low = (wide_w - high.astype(jnp.float32)).astype(jnp.bfloat16)
    extra = jnp.concatenate([high, low, jnp.zeros((local, 128 - 2 * EPG), jnp.bfloat16)], axis=1)
    group = routes[:, 0] // EPG
    place = jnp.arange(local, dtype=jnp.int32)
    earlier = (group[:, None] == group[None, :]) & (place[None, :] < place[:, None])
    slot = group * per + jnp.sum(earlier.astype(jnp.int32), axis=1)
    onehot = (slot[:, None] == place[None, :]).astype(jnp.bfloat16)
    rows = jnp.concatenate([expert_norm, extra], axis=1)
    ordered = lax.dot_general(
        onehot, rows, (((0,), (0,)), ((), ())), preferred_element_type=jnp.float32
    ).astype(jnp.bfloat16)
    z_groups = [[z * EPG + i for z in range(n_groups)] for i in range(EPG)]
    plane_groups = [[z * EPG + i for i in range(EPG)] for z in range(n_groups)]
    arrived = lax.all_to_all(
        ordered, "ep", split_axis=0, concat_axis=0, axis_index_groups=z_groups, tiled=True
    )
    everyone = lax.all_gather(arrived, "ep", axis=0, axis_index_groups=plane_groups, tiled=True)
    all_gate = lax.all_gather(gate_weight[0], "tp", axis=0)
    all_up = lax.all_gather(up_weight[0], "tp", axis=0)
    all_down = lax.all_gather(down_weight[0], "tp", axis=0, tiled=True)
    normal_rows = normed(mixer_input, mixer_gain)
    values = f32dot(normal_rows, value_weight)
    inner = f32dot(normal_rows, inner_gate)
    outer = f32dot(normal_rows, outer_gate)
    mixed_in = (inner * values).astype(jnp.bfloat16)
    padded = padded_2(mixed_in, "ep").astype(jnp.float32)
    conv_sum = (
        kernel_taps[0] * padded[:-2] + kernel_taps[1] * padded[1:-1] + kernel_taps[2] * padded[2:]
    )
    mixer_rows = (outer * conv_sum).astype(jnp.bfloat16)
    partial = f32dot(mixer_rows, mixer_proj).astype(jnp.bfloat16)
    blocks = lax.all_to_all(partial.reshape(split, -1, width), "tp", 0, 0, tiled=True)
    mixer_output = jnp.sum(blocks.astype(jnp.float32), axis=0).astype(jnp.bfloat16)
    tokens = everyone[:, :width]
    mine = lax.axis_index("ep") % EPG
    both = everyone[:, width:].astype(jnp.float32)
    spot = jnp.arange(128, dtype=jnp.int32)
    weight = jnp.sum(
        jnp.where((spot == mine) | (spot == mine + EPG), both, 0.0), axis=1, keepdims=True
    )
    parts = []
    for j in range(split):
        first = f32dot(tokens, all_gate[j])
        second = f32dot(tokens, all_up[j])
        parts.append((jax.nn.silu(first) * second).astype(jnp.bfloat16))
    hidden = jnp.concatenate(parts, axis=1)
    answers = (f32dot(hidden, all_down) * weight).astype(jnp.bfloat16)
    home = lax.psum_scatter(
        answers, "ep", scatter_dimension=0, axis_index_groups=plane_groups, tiled=True
    )
    back = lax.all_to_all(
        home, "ep", split_axis=0, concat_axis=0, axis_index_groups=z_groups, tiled=True
    )
    expert_output = f32dot(onehot, back).astype(jnp.bfloat16)
    return (mixer_output, expert_output)


def solution(mesh):
    in_specs = (
        P("ep", None),
        P(),
        P(None, "tp"),
        P(None, "tp"),
        P(None, "tp"),
        P(None, "tp"),
        P("tp", None),
        P(("ep", "tp"), None),
        P(),
        P(("ep", "tp"), None),
        P(("ep", "tp"), None),
        P(("ep", "tp"), None),
        P("ep", None, "tp"),
        P("ep", None, "tp"),
        P("ep", "tp", None),
    )
    out_specs = (P(("ep", "tp"), None), P(("ep", "tp"), None))
    return jax.shard_map(
        on_device, mesh=mesh, in_specs=in_specs, out_specs=out_specs, check_vma=False
    )
```

profile of v0, /device:TPU:3, one launch (start us, length us, event | category | flops | bytes accessed | tf_op | source)
XLA Modules:
  0.0 350.5 jit_solution(15072283598216035923)
XLA Ops:
  11.8 1.3 fusion.15
  13.4 1.3 fusion.17
  15.6 30.7 %all_to_all.29 = bf16[8,20,2176]{2,1,0:T(8,128)(2,1)S(1)} all-to-all(bf16[8,20,2176]{2,1,0:T(8,128)(2,1)S(1)} %all_to_all.20), channel_id=1, replica_groups={{0,32,64,96,128,160,192,224},{4,36,68,100,132,164,196,228},{8,40,72,104..., dimensions={0} | all-to-all | bytes 1392640 | tf_op jit(solution)/shard_map/all_to_all | solution.py:87
  46.3 1.0 all_to_all.22
  49.5 35.9 %all-gather.6.cloned.1.call-done = bf16[1280,2176]{1,0:T(8,128)(2,1)} async-done(((bf16[160,2176]{1,0:T(8,128)(2,1)}), bf16[1280,2176]{1,0:T(8,128)(2,1)}) %all-gather.6.cloned.1.call-update) | async-done | bytes 5570576 | tf_op jit(solution)/shard_map/all_gather | solution.py:90
  85.4 1.1 select_reduce_fusion
  86.5 51.9 %all-gather.8.cloned.1.call-done = bf16[4,2048,256]{2,1,0:T(8,128)(2,1)} async-done(((bf16[1,2048,256]{2,1,0:T(8,128)(2,1)}), bf16[4,2048,256]{2,1,0:T(8,128)(2,1)}) %all-gather.8.cloned.1.call-update) | async-done | bytes 4194320 | tf_op jit(solution)/shard_map/all_gather | solution.py:91
  138.4 5.5 %fusion.23 = f32[1280,256]{0,1:T(8,128)} fusion(bf16[4,2048,256]{2,1,0:T(8,128)(2,1)} %all-gather.8.cloned.1.call-done, bf16[1280,2176]{1,0:T(8,128)(2,1)} %all-gather.6.cloned.1.call-done), kind=kOutput, calls=%fused_computation.45 | convolution fusion | flops 1342177280 | bytes 7602176 | tf_op jit(solution)/shard_map/dot_general | solution.py:40
  144.6 2.7 fusion.22
  147.3 2.7 fusion.21
  150.0 1.6 fusion.20
  151.6 39.8 %all-gather.10.cloned.1.call-done = bf16[4,2048,256]{2,1,0:T(8,128)(2,1)} async-done(((bf16[1,2048,256]{2,1,0:T(8,128)(2,1)}), bf16[4,2048,256]{2,1,0:T(8,128)(2,1)}) %all-gather.10.cloned.1.call-update) | async-done | bytes 4194320 | tf_op jit(solution)/shard_map/all_gather | solution.py:92
  191.4 5.0 %fusion.11 = bf16[1280,256]{0,1:T(8,128)(2,1)S(1)} fusion(f32[1280,256]{0,1:T(8,128)} %fusion.23, bf16[4,2048,256]{2,1,0:T(8,128)(2,1)} %all-gather.10.cloned.1.call-done, bf16[1280,2176]{1,0:T(8,128)(2,1)} %all-gather.6.cloned.1.call-done), kind=kOutput, calls=%fused_computation.20 | convolution fusion | flops 1344143360 | bytes 8257536 | tf_op jit(solution)/shard_map/dot_general | solution.py:40
  196.4 5.2 %fusion.12 = bf16[1280,256]{0,1:T(8,128)(2,1)} fusion(f32[1280,256]{0,1:T(8,128)S(1)} %copy-done.9, bf16[4,2048,256]{2,1,0:T(8,128)(2,1)S(1)} %copy-done.4, bf16[1280,2176]{1,0:T(8,128)(2,1)} %all-gather.6.cloned.1.call-done), kind=kOutput, calls=%fused_computation.21 | convolution fusion | flops 1344143360 | bytes 8257536 | tf_op jit(solution)/shard_map/dot_general | solution.py:40
  201.7 2.6 fusion.13
  204.3 2.8 fusion.14
  207.1 37.1 %all-gather.12.cloned.1.call-done = bf16[1,1024,2048]{2,1,0:T(8,128)(2,1)} async-done(((bf16[1,256,2048]{2,1,0:T(8,128)(2,1)}), bf16[1,1024,2048]{2,1,0:T(8,128)(2,1)}) %all-gather.12.cloned.1.call-update) | async-done | bytes 4194320 | tf_op jit(solution)/shard_map/all_gather | solution.py:93
  244.2 9.9 %multiply_convert_fusion = bf16[1280,2048]{1,0:T(8,128)(2,1)} fusion(f32[1280]{0:T(1024)S(1)} %select_reduce_fusion, bf16[1,1024,2048]{2,1,0:T(8,128)(2,1)} %all-gather.12.cloned.1.call-done, bf16[1280,256]{0,1:T(8,128)(2,1)} %fusion.14, bf16[1280,256]{0,1:T(8,128)(2,1)} %fusion.13, bf16[1280,256]{0,1:T(8,128)(2,1)} %fusion.12, bf16[1280,256]{0,1:T(8,128)(2,1)S(1)} %fusion.11), kind=kOutput, calls=%fused_computation | convolution fusion | flops 5384437760 | bytes 12063744 | tf_op jit(solution)/shard_map/dot_general | solution.py:40
  254.2 2.3 fusion
  256.5 3.1 fusion.46
  260.6 3.8 %collective-permute-start = (bf16[1,256]{1,0:T(2,128)(2,1)S(1)}, bf16[1,256]{1,0:T(2,128)(2,1)S(1)}, u32[]{:S(2)}, u32[]{:S(2)}) collective-permute-start(bf16[1,256]{1,0:T(2,128)(2,1)S(1)} %get-tuple-element.2), channel_id=1, source_target_pairs={{0,4},{4,8},{8,12},{12,16},{16,20},{20,24},{24,28},{28,32},{32,36}... | collective-permute-start | bytes 1544 | tf_op jit(solution)/shard_map/ppermute | solution.py:17
  264.4 1.9 collective-permute-start.1
  266.3 3.3 collective-permute-done.1
  269.8 6.5 %convolution_convert_fusion.1 = bf16[640,2048]{1,0:T(8,128)(2,1)} fusion(bf16[256,2048]{1,0:T(8,128)(2,1)S(1)} %copy-done, bf16[2048,256]{1,0:T(8,128)(2,1)} %param.19, f32[642,256]{1,0:T(8,128)S(1)} %maximum_convert_fusion, f32[256]{0:T(256)S(1)} %bitcast.59, f32[256]{0:T(256)S(1)} %bitcast.60, f32[256]{0:T(256)S(1)} %bitcast.58, ...), kind=kOutput, calls=%fused_computation.8 | convolution fusion | flops 1349877760 | bytes 9321472 | tf_op jit(solution)/shard_map/dot_general | solution.py:40
  276.3 4.6 %all-to-all-start = ((bf16[4,160,2048]{2,1,0:T(8,128)(2,1)}), bf16[4,160,2048]{2,1,0:T(8,128)(2,1)}, u32[]{:S(2)}, u32[]{:S(2)}) async-start(bf16[4,160,2048]{2,1,0:T(8,128)(2,1)} %bitcast.45), calls=%async_computation | async-start | bytes 5242880 | tf_op jit(solution)/shard_map/all_to_all | solution.py:105
  280.9 13.4 %reduce-scatter.2.cloned.1.call-done = bf16[160,2048]{1,0:T(8,128)(2,1)} async-done(((bf16[1280,2048]{1,0:T(8,128)(2,1)}), bf16[160,2048]{1,0:T(8,128)(2,1)}) %reduce-scatter.2.cloned.1.call-update) | async-done | bytes 655376 | tf_op jit(solution)/shard_map/reduce_scatter | solution.py:121
  294.3 2.0 all_to_all.23
  296.4 15.8 %all-to-all-done = bf16[4,160,2048]{2,1,0:T(8,128)(2,1)} async-done(((bf16[4,160,2048]{2,1,0:T(8,128)(2,1)}), bf16[4,160,2048]{2,1,0:T(8,128)(2,1)}, u32[]{:S(2)}, u32[]{:S(2)}) %all-to-all-start) | async-done | bytes 2621472 | tf_op jit(solution)/shard_map/all_to_all | solution.py:105
  312.2 6.7 %all-to-all-start.2 = ((bf16[8,20,2048]{2,1,0:T(8,128)(2,1)}), bf16[8,20,2048]{2,1,0:T(8,128)(2,1)S(1)}, u32[]{:S(2)}, u32[]{:S(2)}) async-start(bf16[8,20,2048]{2,1,0:T(8,128)(2,1)} %all_to_all.23), calls=%async_computation.3 | async-start | bytes 1572864 | tf_op jit(solution)/shard_map/all_to_all | solution.py:124
  318.9 3.3 reduce_sum.69
  322.1 20.4 %all-to-all-done.2 = bf16[8,20,2048]{2,1,0:T(8,128)(2,1)S(1)} async-done(((bf16[8,20,2048]{2,1,0:T(8,128)(2,1)}), bf16[8,20,2048]{2,1,0:T(8,128)(2,1)S(1)}, u32[]{:S(2)}, u32[]{:S(2)}) %all-to-all-start.2) | async-done | bytes 655392 | tf_op jit(solution)/shard_map/all_to_all | solution.py:124
  342.7 1.2 convolution_convert_fusion.2
  (63 shorter events, 9.7 us)
Async XLA Ops:
  7.2 262.6 %copy-start = (bf16[256,2048]{1,0:T(8,128)(2,1)S(1)}, bf16[256,2048]{1,0:T(8,128)(2,1)}, u32[]{:S(2)}) copy-start(bf16[256,2048]{1,0:T(8,128)(2,1)} %param.21) | copy-start | bytes 3145732
  7.2 78.2 %all-gather.6.cloned.1.call-start = ((), (), s32[]{:S(2)}) async-start(), calls=%async_computation.4 | async-start | bytes 6266880 | tf_op jit(solution)/shard_map/all_gather | solution.py:90
  47.3 91.1 %all-gather.8.cloned.1.call-start = ((), (), s32[]{:S(2)}) async-start(), calls=%async_computation.5 | async-start | bytes 5242880 | tf_op jit(solution)/shard_map/all_gather | solution.py:91
  48.1 143.3 %all-gather.10.cloned.1.call-start = ((), (), s32[]{:S(2)}) async-start(), calls=%async_computation.6 | async-start | bytes 5242880 | tf_op jit(solution)/shard_map/all_gather | solution.py:92
  48.8 195.4 %all-gather.12.cloned.1.call-start = ((), (), s32[]{:S(2)}) async-start(), calls=%async_computation.8 | async-start | bytes 5242880 | tf_op jit(solution)/shard_map/all_gather | solution.py:93
  49.4 244.9 %reduce-scatter.2.cloned.1.call-start = ((), (), s32[]{:S(2)}) async-start(), calls=%async_computation.7 | async-start | bytes 5898240 | tf_op jit(solution)/shard_map/reduce_scatter | solution.py:121
  138.4 5.6 %copy-start.2 = (bf16[1280,2176]{1,0:T(8,128)(2,1)S(1)}, bf16[1280,2176]{1,0:T(8,128)(2,1)}, u32[]{:S(2)}) copy-start(bf16[1280,2176]{1,0:T(8,128)(2,1)} %all-gather.6.cloned.1.call-done) | copy-start | bytes 16711684
  138.4 6.1 %copy-start.5 = (bf16[4,2048,256]{2,1,0:T(8,128)(2,1)S(1)}, bf16[4,2048,256]{2,1,0:T(8,128)(2,1)}, u32[]{:S(2)}) copy-start(bf16[4,2048,256]{2,1,0:T(8,128)(2,1)} %all-gather.8.cloned.1.call-done) | copy-start | bytes 12582916
  191.4 5.0 %copy-start.4 = (bf16[4,2048,256]{2,1,0:T(8,128)(2,1)S(1)}, bf16[4,2048,256]{2,1,0:T(8,128)(2,1)}, u32[]{:S(2)}) copy-start(bf16[4,2048,256]{2,1,0:T(8,128)(2,1)} %all-gather.10.cloned.1.call-done) | copy-start | bytes 12582916
  191.4 5.0 %copy-start.9 = (f32[1280,256]{0,1:T(8,128)S(1)}, f32[1280,256]{0,1:T(8,128)}, u32[]{:S(2)}) copy-start(f32[1280,256]{0,1:T(8,128)} %fusion.22) | copy-start | bytes 3932164
  191.4 10.3 %slice-start = ((s8[5570560]{0:T(1024)(128)(4,1)}), s8[4194304]{0:T(1024)(128)(4,1)S(1)}, s32[]{:S(2)}) async-start(s8[5570560]{0:T(1024)(128)(4,1)} %bitcast.46), calls=%async_computation.9 | async-start | bytes 8388608
  196.4 5.3 %slice-start.1 = ((s8[5570560]{0:T(1024)(128)(4,1)}), s8[1376256]{0:T(1024)(128)(4,1)S(1)}, s32[]{:S(2)}) async-start(s8[5570560]{0:T(1024)(128)(4,1)} %bitcast.46), calls=%async_computation.10 | async-start | bytes 2752512
  196.4 5.3 %copy-start.8 = (f32[1280,256]{0,1:T(8,128)S(1)}, f32[1280,256]{0,1:T(8,128)}, u32[]{:S(2)}) copy-start(f32[1280,256]{0,1:T(8,128)} %fusion.21) | copy-start | bytes 3932164
  254.1 2.4 copy-start.7
  256.5 3.1 copy-start.1
  256.5 3.1 copy-start.6
  259.6 6.7 %copy-start.3 = (f32[3,256]{1,0:T(4,128)S(1)}, f32[3,256]{1,0:T(4,128)}, u32[]{:S(2)}) copy-start(f32[3,256]{1,0:T(4,128)} %param.20) | copy-start | bytes 9220
  260.6 5.8 %collective-permute-start = (bf16[1,256]{1,0:T(2,128)(2,1)S(1)}, bf16[1,256]{1,0:T(2,128)(2,1)S(1)}, u32[]{:S(2)}, u32[]{:S(2)}) collective-permute-start(bf16[1,256]{1,0:T(2,128)(2,1)S(1)} %get-tuple-element.2), channel_id=1, source_target_pairs={{0,4},{4,8},{8,12},{12,16},{16,20},{20,24},{24,28},{28,32},{32,36}... | collective-permute-start | bytes 1544 | tf_op jit(solution)/shard_map/ppermute | solution.py:17
  264.4 5.3 %collective-permute-start.1 = (bf16[1,256]{1,0:T(2,128)(2,1)S(1)}, bf16[1,256]{1,0:T(2,128)(2,1)S(1)}, u32[]{:S(2)}, u32[]{:S(2)}) collective-permute-start(bf16[1,256]{1,0:T(2,128)(2,1)S(1)} %get-tuple-element.3), channel_id=1, source_target_pairs={{4,0},{8,4},{12,8},{16,12},{20,16},{24,20},{28,24},{32,28},{36,32}... | collective-permute-start | bytes 1544 | tf_op jit(solution)/shard_map/ppermute | solution.py:19
  276.3 35.9 %all-to-all-start = ((bf16[4,160,2048]{2,1,0:T(8,128)(2,1)}), bf16[4,160,2048]{2,1,0:T(8,128)(2,1)}, u32[]{:S(2)}, u32[]{:S(2)}) async-start(bf16[4,160,2048]{2,1,0:T(8,128)(2,1)} %bitcast.45), calls=%async_computation | async-start | bytes 5242880 | tf_op jit(solution)/shard_map/all_to_all | solution.py:105
  312.2 30.4 %all-to-all-start.2 = ((bf16[8,20,2048]{2,1,0:T(8,128)(2,1)}), bf16[8,20,2048]{2,1,0:T(8,128)(2,1)S(1)}, u32[]{:S(2)}, u32[]{:S(2)}) async-start(bf16[8,20,2048]{2,1,0:T(8,128)(2,1)} %all_to_all.23), calls=%async_computation.3 | async-start | bytes 1572864 | tf_op jit(solution)/shard_map/all_to_all | solution.py:124
Sparse Core Ops, SparseCore 0:
  47.5 37.8 all-gather.5
  87.2 51.2 all-gather.7
  140.2 51.1 all-gather.9
  193.1 51.1 all-gather.11
  254.3 40.0 reduce-scatter.1
where the time goes:
time: 351 us; the launch traced here: 350 us
  waiting for transfers between devices  220 us (63%)
  matrix products  50.3 us (14%)
  blocking collectives  30.7 us (9%)
  starting transfers between devices  17.3 us (5%)
  between operations  14.1 us (4%)
  other arithmetic  13.2 us (4%)
  local copies, waits for them, and re-layouts  5.27 us (2%)
    all_gather x1, waiting for transfers between devices, on_device(): all_gate = lax.all_gather(gate_weight[0], 'tp', axis=0)  51.9 us
    dot_general x13, matrix products, f32dot(): return jnp.dot(a, b, preferred_element_type=jnp.float32)  49.9 us
    all_gather x1, waiting for transfers between devices, on_device(): all_up = lax.all_gather(up_weight[0], 'tp', axis=0)  39.8 us
    all_gather x1, waiting for transfers between devices, on_device(): all_down = lax.all_gather(down_weight[0], 'tp', axis=0, tiled=True)  37.1 us
    all_gather x1, waiting for transfers between devices, on_device(): lax.all_gather(arrived, 'ep', axis=0, axis_index_groups=plane_groups, til...  35.9 us
    all_to_all x1, blocking collectives, on_device(): lax.all_to_all(ordered, 'ep', split_axis=0, concat_axis=0, axis_index_gro...  30.7 us
    all_to_all x1, waiting for transfers between devices, on_device(): lax.all_to_all(home, 'ep', split_axis=0, concat_axis=0, axis_index_groups...  20.4 us
    all_to_all x1, waiting for transfers between devices, on_device(): lax.all_to_all(partial.reshape(split, -1, width), 'tp', 0, 0, tiled=True)  15.8 us
  transfers between devices with their start and end apart: 9, of which 8 were waited for; matrix products, arithmetic and copies ran while one was open for 13% of the time, Pallas kernels for 0%

commit v1 on v0

--- a/solution.py
+++ b/solution.py
@@ -5,6 +5,11 @@
 
 EPG = 8
 EPSILON = 1e-06
+
+
+def gather_by_exchange(array, axis, dim):
+    copies = jnp.concatenate([array] * lax.axis_size(axis), axis=dim)
+    return lax.all_to_all(copies, axis, dim, dim, tiled=True)
 
 
 def padded_2(cells, axis):
@@ -90,7 +95,7 @@
     everyone = lax.all_gather(arrived, "ep", axis=0, axis_index_groups=plane_groups, tiled=True)
     all_gate = lax.all_gather(gate_weight[0], "tp", axis=0)
     all_up = lax.all_gather(up_weight[0], "tp", axis=0)
-    all_down = lax.all_gather(down_weight[0], "tp", axis=0, tiled=True)
+    all_down = gather_by_exchange(down_weight[0], "tp", 0)
     normal_rows = normed(mixer_input, mixer_gain)
     values = f32dot(normal_rows, value_weight)
     inner = f32dot(normal_rows, inner_gate)

time: 351 us -> 290 us (0.83)
  waiting for transfers between devices: 220 us -> 147 us
  starting transfers between devices: 17.3 us -> 22.3 us
    all_gather x1, waiting for transfers between devices: 51.9 us -> 5.95 us  [on_device(): all_gate = lax.all_gather(gate_weight[0], 'tp', axis=0)]
    all_gather x1 -> x0, waiting for transfers between devices: 37.1 us -> none  [on_device(): all_down = lax.all_gather(down_weight[0], 'tp', axis=0, tiled=True)]
    all_gather x1, waiting for transfers between devices: 35.9 us -> 47.4 us  [on_device(): lax.all_gather(arrived, 'ep', axis=0, axis_index_groups=plane_groups, til...]
    all_to_all x0 -> x1, starting transfers between devices: none -> 4.87 us  [gather_by_exchange(): return lax.all_to_all(copies, axis, dim, dim, tiled=True)]
    concatenate x0 -> x1, other arithmetic: none -> 4.09 us  [gather_by_exchange(): copies = jnp.concatenate([array] * lax.axis_size(axis), axis=dim)]
  transfers between devices with their start and end apart: 9 -> 9, of which waited for: 8 -> 7; matrix products, arithmetic and copies ran while one was open for 13% -> 21% of each run, Pallas kernels for 0% -> 0%
where the time goes in v1:
time: 290 us; the launch traced here: 289 us
  waiting for transfers between devices  147 us (51%)
  matrix products  52.9 us (18%)
  blocking collectives  30.7 us (11%)
  starting transfers between devices  22.3 us (8%)
  other arithmetic  16.3 us (6%)
  between operations  14 us (5%)
  local copies, waits for them, and re-layouts  5.28 us (2%)
    dot_general x13, matrix products, f32dot(): return jnp.dot(a, b, preferred_element_type=jnp.float32)  52.4 us
    all_gather x1, waiting for transfers between devices, on_device(): lax.all_gather(arrived, 'ep', axis=0, axis_index_groups=plane_groups, til...  47.4 us
    all_gather x1, waiting for transfers between devices, on_device(): all_up = lax.all_gather(up_weight[0], 'tp', axis=0)  39.7 us
    all_to_all x1, blocking collectives, on_device(): lax.all_to_all(ordered, 'ep', split_axis=0, concat_axis=0, axis_index_gro...  30.7 us
    all_to_all x1, waiting for transfers between devices, on_device(): lax.all_to_all(home, 'ep', split_axis=0, concat_axis=0, axis_index_groups...  20.4 us
    all_to_all x1, waiting for transfers between devices, on_device(): lax.all_to_all(partial.reshape(split, -1, width), 'tp', 0, 0, tiled=True)  15.8 us
    reduce_scatter x1, waiting for transfers between devices, on_device(): lax.psum_scatter(answers, 'ep', scatter_dimension=0, axis_index_groups=pl...  13.4 us
    all_to_all x1, starting transfers between devices, on_device(): lax.all_to_all(home, 'ep', split_axis=0, concat_axis=0, axis_index_groups...  6.72 us
  transfers between devices with their start and end apart: 9, of which 7 were waited for; matrix products, arithmetic and copies ran while one was open for 21% of the time, Pallas kernels for 0%

profile of v1, /device:TPU:3, one launch (start us, length us, event | category | flops | bytes accessed | tf_op | source)
XLA Modules:
  0.0 289.0 jit_solution(1430096890312880267)
XLA Ops:
  12.5 1.3 fusion.14
  13.8 1.3 fusion.16
  16.3 30.7 %all_to_all.41 = bf16[8,20,2176]{2,1,0:T(8,128)(2,1)S(1)} all-to-all(bf16[8,20,2176]{2,1,0:T(8,128)(2,1)S(1)} %all_to_all.28), channel_id=1, replica_groups={{0,32,64,96,128,160,192,224},{4,36,68,100,132,164,196,228},{8,40,72,104..., dimensions={0} | all-to-all | bytes 1392640 | tf_op jit(solution)/shard_map/all_to_all | solution.py:92
  47.0 1.0 all_to_all.30
  48.8 4.1 %pad_maximum_fusion = bf16[1024,2048]{1,0:T(8,128)(2,1)} fusion(bf16[256,2048]{1,0:T(8,128)(2,1)} %bitcast.48), kind=kLoop, calls=%fused_computation.6 | loop fusion | flops 16777216 | bytes 5242880 | tf_op jit(solution)/shard_map/concatenate | solution.py:11
  52.9 4.9 %all-to-all-start.2 = ((bf16[4,256,2048]{2,1,0:T(8,128)(2,1)}), bf16[4,256,2048]{2,1,0:T(8,128)(2,1)}, u32[]{:S(2)}, u32[]{:S(2)}) async-start(bf16[4,256,2048]{2,1,0:T(8,128)(2,1)} %bitcast.46), calls=%async_computation.2 | async-start | bytes 8388608 | tf_op jit(solution)/shard_map/all_to_all | solution.py:12
  58.0 6.0 %all-gather.6.cloned.1.call-done = bf16[4,2048,256]{2,1,0:T(8,128)(2,1)} async-done(((bf16[1,2048,256]{2,1,0:T(8,128)(2,1)}), bf16[4,2048,256]{2,1,0:T(8,128)(2,1)}) %all-gather.6.cloned.1.call-update) | async-done | bytes 4194320 | tf_op jit(solution)/shard_map/all_gather | solution.py:96
  64.0 47.4 %all-gather.4.cloned.1.call-done = bf16[1280,2176]{1,0:T(8,128)(2,1)} async-done(((bf16[160,2176]{1,0:T(8,128)(2,1)}), bf16[1280,2176]{1,0:T(8,128)(2,1)}) %all-gather.4.cloned.1.call-update) | async-done | bytes 5570576 | tf_op jit(solution)/shard_map/all_gather | solution.py:95
  111.4 5.5 %fusion.22 = f32[1280,256]{0,1:T(8,128)} fusion(bf16[4,2048,256]{2,1,0:T(8,128)(2,1)} %all-gather.6.cloned.1.call-done, bf16[1280,2176]{1,0:T(8,128)(2,1)} %all-gather.4.cloned.1.call-done), kind=kOutput, calls=%fused_computation.45 | convolution fusion | flops 1342177280 | bytes 7602176 | tf_op jit(solution)/shard_map/dot_general | solution.py:45
  117.5 2.7 fusion.21
  120.2 2.7 fusion.20
  122.9 1.6 fusion.19
  124.7 39.7 %all-gather.8.cloned.1.call-done = bf16[4,2048,256]{2,1,0:T(8,128)(2,1)} async-done(((bf16[1,2048,256]{2,1,0:T(8,128)(2,1)}), bf16[4,2048,256]{2,1,0:T(8,128)(2,1)}) %all-gather.8.cloned.1.call-update) | async-done | bytes 4194320 | tf_op jit(solution)/shard_map/all_gather | solution.py:97
  164.4 5.0 %fusion.10 = bf16[1280,256]{0,1:T(8,128)(2,1)S(1)} fusion(f32[1280,256]{0,1:T(8,128)} %fusion.22, bf16[4,2048,256]{2,1,0:T(8,128)(2,1)} %all-gather.8.cloned.1.call-done, bf16[1280,2176]{1,0:T(8,128)(2,1)} %all-gather.4.cloned.1.call-done), kind=kOutput, calls=%fused_computation.20 | convolution fusion | flops 1344143360 | bytes 8257536 | tf_op jit(solution)/shard_map/dot_general | solution.py:45
  169.4 5.2 %fusion.11 = bf16[1280,256]{0,1:T(8,128)(2,1)} fusion(f32[1280,256]{0,1:T(8,128)S(1)} %copy-done.9, bf16[4,2048,256]{2,1,0:T(8,128)(2,1)S(1)} %copy-done.5, bf16[1280,2176]{1,0:T(8,128)(2,1)} %all-gather.4.cloned.1.call-done), kind=kOutput, calls=%fused_computation.21 | convolution fusion | flops 1344143360 | bytes 8257536 | tf_op jit(solution)/shard_map/dot_general | solution.py:45
  174.7 5.2 %fusion.12 = bf16[1280,256]{0,1:T(8,128)(2,1)} fusion(f32[1280,256]{0,1:T(8,128)S(1)} %copy-done.8, bf16[4,2048,256]{2,1,0:T(8,128)(2,1)S(1)} %copy-done.5, bf16[1280,2176]{1,0:T(8,128)(2,1)} %all-gather.4.cloned.1.call-done), kind=kOutput, calls=%fused_computation.22 | convolution fusion | flops 1344143360 | bytes 8257536 | tf_op jit(solution)/shard_map/dot_general | solution.py:45
  179.9 2.9 fusion.13
  182.7 9.9 %multiply_convert_fusion = bf16[1280,2048]{1,0:T(8,128)(2,1)} fusion(bf16[1024,2048]{1,0:T(8,128)(2,1)} %bitcast.22, f32[1280]{0:T(1024)S(1)} %select_reduce_fusion, bf16[1280,256]{0,1:T(8,128)(2,1)} %fusion.13, bf16[1280,256]{0,1:T(8,128)(2,1)} %fusion.12, bf16[1280,256]{0,1:T(8,128)(2,1)} %fusion.11, bf16[1280,256]{0,1:T(8,128)(2,1)S(1)} %fusion.10), kind=kOutput, calls=%fused_computation | convolution fusion | flops 5384437760 | bytes 12063744 | tf_op jit(solution)/shard_map/dot_general | solution.py:45
  192.7 2.3 fusion
  195.0 3.1 %fusion.45 = f32[640,256]{1,0:T(8,128)S(1)} fusion(bf16[2048,256]{1,0:T(8,128)(2,1)} %param.18, bf16[640,2048]{1,0:T(8,128)(2,1)} %param.15, f32[2048]{0:T(1024)S(1)} %copy-done.7, f32[640]{0:T(1024)S(1)} %add_rsqrt_fusion), kind=kOutput, calls=%fused_computation.97 | convolution fusion | flops 676331520 | bytes 4336128 | tf_op jit(solution)/shard_map/dot_general | solution.py:45
  199.1 3.8 %collective-permute-start = (bf16[1,256]{1,0:T(2,128)(2,1)S(1)}, bf16[1,256]{1,0:T(2,128)(2,1)S(1)}, u32[]{:S(2)}, u32[]{:S(2)}) collective-permute-start(bf16[1,256]{1,0:T(2,128)(2,1)S(1)} %get-tuple-element.2), channel_id=1, source_target_pairs={{0,4},{4,8},{8,12},{12,16},{16,20},{20,24},{24,28},{28,32},{32,36}... | collective-permute-start | bytes 1544 | tf_op jit(solution)/shard_map/ppermute | solution.py:22
  202.9 1.9 collective-permute-start.1
  204.9 3.3 %collective-permute-done.1 = bf16[1,256]{1,0:T(2,128)(2,1)S(1)} collective-permute-done((bf16[1,256]{1,0:T(2,128)(2,1)S(1)}, bf16[1,256]{1,0:T(2,128)(2,1)S(1)}, u32[]{:S(2)}, u32[]{:S(2)}) %collective-permute-start.1) | collective-permute-done | bytes 544 | tf_op jit(solution)/shard_map/ppermute | solution.py:24
  208.3 6.5 %convolution_convert_fusion.1 = bf16[640,2048]{1,0:T(8,128)(2,1)} fusion(bf16[256,2048]{1,0:T(8,128)(2,1)S(1)} %copy-done, bf16[2048,256]{1,0:T(8,128)(2,1)} %param.19, f32[642,256]{1,0:T(8,128)S(1)} %maximum_convert_fusion, f32[256]{0:T(256)S(1)} %bitcast.62, f32[256]{0:T(256)S(1)} %bitcast.63, f32[256]{0:T(256)S(1)} %bitcast.61, ...), kind=kOutput, calls=%fused_computation.8 | convolution fusion | flops 1349877760 | bytes 9321472 | tf_op jit(solution)/shard_map/dot_general | solution.py:45
  214.8 4.6 %all-to-all-start = ((bf16[4,160,2048]{2,1,0:T(8,128)(2,1)}), bf16[4,160,2048]{2,1,0:T(8,128)(2,1)}, u32[]{:S(2)}, u32[]{:S(2)}) async-start(bf16[4,160,2048]{2,1,0:T(8,128)(2,1)} %bitcast.47), calls=%async_computation | async-start | bytes 5242880 | tf_op jit(solution)/shard_map/all_to_all | solution.py:110
  219.4 13.4 %reduce-scatter.2.cloned.1.call-done = bf16[160,2048]{1,0:T(8,128)(2,1)} async-done(((bf16[1280,2048]{1,0:T(8,128)(2,1)}), bf16[160,2048]{1,0:T(8,128)(2,1)}) %reduce-scatter.2.cloned.1.call-update) | async-done | bytes 655376 | tf_op jit(solution)/shard_map/reduce_scatter | solution.py:126
  232.9 2.0 all_to_all.34
  234.9 15.8 %all-to-all-done = bf16[4,160,2048]{2,1,0:T(8,128)(2,1)} async-done(((bf16[4,160,2048]{2,1,0:T(8,128)(2,1)}), bf16[4,160,2048]{2,1,0:T(8,128)(2,1)}, u32[]{:S(2)}, u32[]{:S(2)}) %all-to-all-start) | async-done | bytes 2621472 | tf_op jit(solution)/shard_map/all_to_all | solution.py:110
  250.7 6.7 %all-to-all-start.3 = ((bf16[8,20,2048]{2,1,0:T(8,128)(2,1)}), bf16[8,20,2048]{2,1,0:T(8,128)(2,1)S(1)}, u32[]{:S(2)}, u32[]{:S(2)}) async-start(bf16[8,20,2048]{2,1,0:T(8,128)(2,1)} %all_to_all.34), calls=%async_computation.4 | async-start | bytes 1572864 | tf_op jit(solution)/shard_map/all_to_all | solution.py:129
  257.4 3.3 %reduce_sum.69 = bf16[160,2048]{1,0:T(8,128)(2,1)} reduce(bf16[4,160,2048]{2,1,0:T(8,128)(2,1)} %all-to-all-done, bf16[]{:T(256)} %constant.55.clone.1), dimensions={0}, to_apply=%region_1.2 | reduce | flops 983040 | bytes 3276802 | tf_op jit(solution)/shard_map/reduce_sum | solution.py:111
  260.7 20.4 %all-to-all-done.3 = bf16[8,20,2048]{2,1,0:T(8,128)(2,1)S(1)} async-done(((bf16[8,20,2048]{2,1,0:T(8,128)(2,1)}), bf16[8,20,2048]{2,1,0:T(8,128)(2,1)S(1)}, u32[]{:S(2)}, u32[]{:S(2)}) %all-to-all-start.3) | async-done | bytes 655392 | tf_op jit(solution)/shard_map/all_to_all | solution.py:129
  281.2 1.2 convolution_convert_fusion.2
  (63 shorter events, 9.4 us)
Async XLA Ops:
  7.2 201.1 %copy-start = (bf16[256,2048]{1,0:T(8,128)(2,1)S(1)}, bf16[256,2048]{1,0:T(8,128)(2,1)}, u32[]{:S(2)}) copy-start(bf16[256,2048]{1,0:T(8,128)(2,1)} %param.21) | copy-start | bytes 3145732
  7.2 56.8 %all-gather.6.cloned.1.call-start = ((), (), s32[]{:S(2)}) async-start(), calls=%async_computation.6 | async-start | bytes 5242880 | tf_op jit(solution)/shard_map/all_gather | solution.py:96
  7.9 103.4 %all-gather.4.cloned.1.call-start = ((), (), s32[]{:S(2)}) async-start(), calls=%async_computation.5 | async-start | bytes 6266880 | tf_op jit(solution)/shard_map/all_gather | solution.py:95
  48.0 116.4 %all-gather.8.cloned.1.call-start = ((), (), s32[]{:S(2)}) async-start(), calls=%async_computation.7 | async-start | bytes 5242880 | tf_op jit(solution)/shard_map/all_gather | solution.py:97
  52.9 129.9 %all-to-all-start.2 = ((bf16[4,256,2048]{2,1,0:T(8,128)(2,1)}), bf16[4,256,2048]{2,1,0:T(8,128)(2,1)}, u32[]{:S(2)}, u32[]{:S(2)}) async-start(bf16[4,256,2048]{2,1,0:T(8,128)(2,1)} %bitcast.46), calls=%async_computation.2 | async-start | bytes 8388608 | tf_op jit(solution)/shard_map/all_to_all | solution.py:12
  57.7 175.1 %reduce-scatter.2.cloned.1.call-start = ((), (), s32[]{:S(2)}) async-start(), calls=%async_computation.8 | async-start | bytes 5898240 | tf_op jit(solution)/shard_map/reduce_scatter | solution.py:126
  111.4 5.6 %copy-start.2 = (bf16[1280,2176]{1,0:T(8,128)(2,1)S(1)}, bf16[1280,2176]{1,0:T(8,128)(2,1)}, u32[]{:S(2)}) copy-start(bf16[1280,2176]{1,0:T(8,128)(2,1)} %all-gather.4.cloned.1.call-done) | copy-start | bytes 16711684
  111.4 6.1 %copy-start.4 = (bf16[4,2048,256]{2,1,0:T(8,128)(2,1)S(1)}, bf16[4,2048,256]{2,1,0:T(8,128)(2,1)}, u32[]{:S(2)}) copy-start(bf16[4,2048,256]{2,1,0:T(8,128)(2,1)} %all-gather.6.cloned.1.call-done) | copy-start | bytes 12582916
  164.4 5.0 %copy-start.5 = (bf16[4,2048,256]{2,1,0:T(8,128)(2,1)S(1)}, bf16[4,2048,256]{2,1,0:T(8,128)(2,1)}, u32[]{:S(2)}) copy-start(bf16[4,2048,256]{2,1,0:T(8,128)(2,1)} %all-gather.8.cloned.1.call-done) | copy-start | bytes 12582916
  164.4 5.0 %copy-start.9 = (f32[1280,256]{0,1:T(8,128)S(1)}, f32[1280,256]{0,1:T(8,128)}, u32[]{:S(2)}) copy-start(f32[1280,256]{0,1:T(8,128)} %fusion.21) | copy-start | bytes 3932164
  169.4 5.2 %copy-start.8 = (f32[1280,256]{0,1:T(8,128)S(1)}, f32[1280,256]{0,1:T(8,128)}, u32[]{:S(2)}) copy-start(f32[1280,256]{0,1:T(8,128)} %fusion.20) | copy-start | bytes 3932164
  169.4 10.4 %slice-start = ((s8[5570560]{0:T(1024)(128)(4,1)}), s8[4194304]{0:T(1024)(128)(4,1)S(1)}, s32[]{:S(2)}) async-start(s8[5570560]{0:T(1024)(128)(4,1)} %bitcast.49), calls=%async_computation.9 | async-start | bytes 8388608
  174.7 5.2 %slice-start.1 = ((s8[5570560]{0:T(1024)(128)(4,1)}), s8[1376256]{0:T(1024)(128)(4,1)S(1)}, s32[]{:S(2)}) async-start(s8[5570560]{0:T(1024)(128)(4,1)} %bitcast.49), calls=%async_computation.10 | async-start | bytes 2752512
  192.7 2.4 copy-start.7
  195.0 3.1 %copy-start.1 = (bf16[640,2048]{1,0:T(8,128)(2,1)S(1)}, bf16[640,2048]{1,0:T(8,128)(2,1)}, u32[]{:S(2)}) copy-start(bf16[640,2048]{1,0:T(8,128)(2,1)} %param.15) | copy-start | bytes 7864324
  195.0 3.1 %copy-start.6 = (bf16[2048,256]{1,0:T(8,128)(2,1)S(1)}, bf16[2048,256]{1,0:T(8,128)(2,1)}, u32[]{:S(2)}) copy-start(bf16[2048,256]{1,0:T(8,128)(2,1)} %param.17) | copy-start | bytes 3145732
  198.1 6.7 %copy-start.3 = (f32[3,256]{1,0:T(4,128)S(1)}, f32[3,256]{1,0:T(4,128)}, u32[]{:S(2)}) copy-start(f32[3,256]{1,0:T(4,128)} %param.20) | copy-start | bytes 9220
  199.1 5.8 %collective-permute-start = (bf16[1,256]{1,0:T(2,128)(2,1)S(1)}, bf16[1,256]{1,0:T(2,128)(2,1)S(1)}, u32[]{:S(2)}, u32[]{:S(2)}) collective-permute-start(bf16[1,256]{1,0:T(2,128)(2,1)S(1)} %get-tuple-element.2), channel_id=1, source_target_pairs={{0,4},{4,8},{8,12},{12,16},{16,20},{20,24},{24,28},{28,32},{32,36}... | collective-permute-start | bytes 1544 | tf_op jit(solution)/shard_map/ppermute | solution.py:22
  202.9 5.3 %collective-permute-start.1 = (bf16[1,256]{1,0:T(2,128)(2,1)S(1)}, bf16[1,256]{1,0:T(2,128)(2,1)S(1)}, u32[]{:S(2)}, u32[]{:S(2)}) collective-permute-start(bf16[1,256]{1,0:T(2,128)(2,1)S(1)} %get-tuple-element.3), channel_id=1, source_target_pairs={{4,0},{8,4},{12,8},{16,12},{20,16},{24,20},{28,24},{32,28},{36,32}... | collective-permute-start | bytes 1544 | tf_op jit(solution)/shard_map/ppermute | solution.py:24
  214.8 35.9 %all-to-all-start = ((bf16[4,160,2048]{2,1,0:T(8,128)(2,1)}), bf16[4,160,2048]{2,1,0:T(8,128)(2,1)}, u32[]{:S(2)}, u32[]{:S(2)}) async-start(bf16[4,160,2048]{2,1,0:T(8,128)(2,1)} %bitcast.47), calls=%async_computation | async-start | bytes 5242880 | tf_op jit(solution)/shard_map/all_to_all | solution.py:110
  250.7 30.4 %all-to-all-start.3 = ((bf16[8,20,2048]{2,1,0:T(8,128)(2,1)}), bf16[8,20,2048]{2,1,0:T(8,128)(2,1)S(1)}, u32[]{:S(2)}, u32[]{:S(2)}) async-start(bf16[8,20,2048]{2,1,0:T(8,128)(2,1)} %all_to_all.34), calls=%async_computation.4 | async-start | bytes 1572864 | tf_op jit(solution)/shard_map/all_to_all | solution.py:129
Sparse Core Ops, SparseCore 0:
  9.8 54.1 all-gather.5
  65.8 45.5 all-gather.3
  113.2 51.1 all-gather.7
  192.8 40.0 reduce-scatter.1
